TPU v7x, 32 devices: a whole 2x2x4 slice. The times are simulated.
32 devices in a mesh: st: 16 (over z, y, x), tp: 2 (over core).
Axes of the slice: x: 2, y: 2, z: 4, core: 2. Of those that a mesh axis runs over, the one named last changes fastest.
Arguments:
- tokens: bfloat16 [16384, 2048], P('st', 'tp'), may hold values from -6 to 6
- passage_ids: int32 [256, 2], P('st'), may hold values from 0 to 255, as said below
- passage_store: bfloat16 [256, 64, 2048], P('st'), may hold values from -6 to 6
- norm_gain: bfloat16 [2048], replicated, may hold values from 0.099609375 to 1.8984375
- conv_value_weight: bfloat16 [2048, 1536], P(None, 'tp'), may hold values from -0.125 to 0.125
- conv_gate_weight: bfloat16 [2048, 1536], P(None, 'tp'), may hold values from -0.125 to 0.125
- conv_weight: bfloat16 [31, 1536], P(None, 'tp'), may hold values from -1 to 1
- ln_gain: bfloat16 [1536], P('tp'), may hold values from 0.099609375 to 1.8984375
- query_weight: bfloat16 [2048, 512], P(None, 'tp'), may hold values from -0.125 to 0.125
- query_gain: bfloat16 [512], P('tp'), may hold values from 0.5 to 10
- passage_gain: bfloat16 [2048], replicated, may hold values from 0.099609375 to 1.8984375
- key_weight: bfloat16 [2048, 512], P(None, 'tp'), may hold values from -0.125 to 0.125
- value_weight: bfloat16 [2048, 512], P(None, 'tp'), may hold values from -0.125 to 0.125
- key_gain: bfloat16 [512], P('tp'), may hold values from 0.5 to 10
- memory_gate: bfloat16 [512], P('tp'), may hold values from 0.29882812 to 1.5
- conv_out_weight: bfloat16 [1536, 2048], P('tp'), may hold values from -0.125 to 0.125
- memory_out_weight: bfloat16 [512, 2048], P('tp'), may hold values from -0.125 to 0.125
Outputs:
- layer_out: bfloat16 [16384, 2048], P(('st', 'tp'))
Inputs may be any that keep to these rules, and one draw needn't show every extreme that they name: The owner of passage p is p // 16. Among the 32 entries of the rows of passage_ids that lie on one index of st (aligned runs of 16 rows, that is the blocks of one index of st), no owner is named more than 4 times, and in every such run some owner is named exactly 4 times.
All inputs are finite; a program needn't handle non-finite values.
Results may differ from a plain program's by a relative error of at most 0.008.
The roundings to bfloat16 on the way count: a program that leaves them out, or rounds other values in their place, can miss the bound.
Values may be sent and summed in bfloat16 or wider, within the bound.
A program may use at most 192 MiB of HBM per device.

v0:
```python
import functools

import jax
import jax.numpy as jnp
from jax import lax
from jax.experimental import pallas as pl
from jax.experimental.pallas import tpu as pltpu
from jax.sharding import PartitionSpec as P

C_A = 1536
MEM_HD = 64
SEQS_DEV = 2
NORM_EPS = 1e-06
LAYER_EPS = 1e-05
REACH = 2
MESH = pl.DeviceIdType.MESH
OFFSETS = tuple(range(-REACH, REACH + 1))


def head_norm(product, gain_row):
    lane = lax.broadcasted_iota(jnp.int32, product.shape, 1)
    squares = product * product
    scale = jnp.zeros_like(product)
    for head in range(product.shape[1] // MEM_HD):
        inside = (lane >= head * MEM_HD) & (lane < (head + 1) * MEM_HD)
        total = jnp.sum(jnp.where(inside, squares, 0.0), axis=-1, keepdims=True)
        scale = jnp.where(inside, lax.rsqrt(total * (1.0 / MEM_HD) + NORM_EPS), scale)
    return (product * scale * gain_row.astype(jnp.float32)).astype(jnp.bfloat16)


def dot32(left, right):
    return jnp.dot(left, right, preferred_element_type=jnp.float32)


def row_norm(rows, gain_row):
    wide = rows.astype(jnp.float32)
    factor = lax.rsqrt(jnp.mean(wide * wide, axis=-1, keepdims=True) + NORM_EPS)
    return (wide * factor * gain_row.astype(jnp.float32)).astype(jnp.bfloat16)


def split_axis(count):
    plane = 1
    for size in range(1, count + 1):
        if count % size == 0 and size * size <= count:
            plane = size
    return count // plane, plane


def layer_kernel(
    depth,
    plane,
    most,
    passes,
    slots_ref,
    wanted_smem,
    wanted_ref,
    norm_gain_ref,
    passage_gain_ref,
    key_gain_ref,
    query_gain_ref,
    ln_gain_ref,
    gate_ref,
    taps_ref,
    tokens_hbm,
    store_hbm,
    key_w_hbm,
    value_w_hbm,
    query_w_hbm,
    conv_value_hbm,
    conv_gate_hbm,
    conv_out_hbm,
    mem_out_hbm,
    out_hbm,
    key_w,
    value_w,
    query_w,
    conv_value,
    conv_gate,
    conv_out_w,
    mem_out_w,
    store_buf,
    x_buf,
    padded,
    filtered,
    acc,
    queries,
    memory,
    stats,
    stats_in,
    part_out,
    part_in,
    result,
    ids_in,
    ids_smem,
    slots,
    *rest,
):
    columns, rest = dict(zip(OFFSETS, rest[: len(OFFSETS)])), rest[len(OFFSETS) :]
    (
        picked,
        far_picked,
        load_sem,
        store_sem,
        x_sem,
        ids_copy_sem,
        ids_send,
        ids_recv,
        hop_send,
        hop_recv,
        plane_send,
        plane_recv,
        far_send,
        far_recv,
        tp_send,
        tp_recv,
        out_sem,
    ) = rest
    me = lax.axis_index("st")
    tp = lax.axis_index("tp")
    z, p = me // plane, me % plane
    power = plane & (plane - 1) == 0
    passage_len = slots.shape[3]
    store_size = columns[0].shape[0]
    tile_passages = store_buf.shape[1] // passage_len
    tiles = store_size // tile_passages
    tile_rows = tile_passages * passage_len
    tokens, features = x_buf.shape
    half = features // 2
    width = key_w.shape[1]

    def reader_place(step):
        return p ^ step if power else (p + step) % plane

    def asker_place(step):
        return p ^ step if power else (p - step + plane) % plane

    far_planes = [o for o in range(depth) if max(o, depth - 1 - o) > REACH]

    def is_far(other):
        return jnp.abs(other - z) > REACH

    def store_copy(tile):
        return pltpu.make_async_copy(
            store_hbm.at[pl.ds(tile * tile_rows, tile_rows)],
            store_buf.at[tile],
            store_sem.at[tile],
        )

    loads = [
        pltpu.make_async_copy(src, dst, load_sem.at[number])
        for number, (src, dst) in enumerate(
            [
                (key_w_hbm, key_w),
                (value_w_hbm, value_w),
                (query_w_hbm, query_w),
                (conv_value_hbm, conv_value),
                (conv_gate_hbm, conv_gate),
                (conv_out_hbm, conv_out_w),
                (mem_out_hbm, mem_out_w),
            ]
        )
    ]
    mine = pl.ds(pl.multiple_of(tp * half, half), half)
    x_copy = pltpu.make_async_copy(tokens_hbm, x_buf.at[:, mine], x_sem)
    store_copy(0).start()
    loads[0].start()
    loads[1].start()
    for tile in range(1, tiles):
        store_copy(tile).start()
    x_copy.start()
    for load in loads[2:]:
        load.start()

    barrier = pltpu.get_barrier_semaphore()

    def greet(st, core):
        pl.semaphore_signal(barrier, inc=1, device_id=(st, core), device_id_type=MESH)

    greet(me, 1 - tp)
    for step in range(1, plane):
        greet(z * plane + reader_place(step), tp)

    @pl.when(z > 0)
    def _():
        greet(me - plane, tp)

    @pl.when(z < depth - 1)
    def _():
        greet(me + plane, tp)

    met = 1 + plane - 1 + jnp.where(z > 0, 1, 0) + jnp.where(z < depth - 1, 1, 0)
    for other in far_planes:

        @pl.when(is_far(other))
        def _(other=other):
            for place in range(plane):
                greet(other * plane + place, tp)

        met = met + jnp.where(is_far(other), plane, 0)
    pl.semaphore_wait(barrier, met)

    def ids_copy(st, send_slot):
        return pltpu.make_async_remote_copy(
            src_ref=wanted_ref,
            dst_ref=ids_in.at[me],
            send_sem=ids_send.at[send_slot],
            recv_sem=ids_recv.at[me],
            device_id=(st, tp),
            device_id_type=MESH,
        )

    def ids_arrival(st):
        return pltpu.make_async_remote_copy(
            src_ref=wanted_ref,
            dst_ref=ids_in.at[st],
            send_sem=ids_send.at[st],
            recv_sem=ids_recv.at[st],
            device_id=(st, tp),
            device_id_type=MESH,
        )

    def ids_local(st):
        return pltpu.make_async_copy(ids_in.at[st], ids_smem.at[st], ids_copy_sem.at[st])

    def for_askers(action):
        for step in range(1, plane):
            action(z * plane + reader_place(step))
        for other in far_planes:

            @pl.when(is_far(other))
            def _(other=other):
                for place in range(plane):
                    action(other * plane + place)

    for_askers(lambda st: ids_copy(st, st).start())

    swap = pltpu.make_async_remote_copy(
        src_ref=tokens_hbm,
        dst_ref=x_buf.at[:, mine],
        send_sem=tp_send.at[0],
        recv_sem=tp_recv.at[0],
        device_id=(me, 1 - tp),
        device_id_type=MESH,
    )
    swap.start()

    def hop(level, up, tile):
        source = columns[-level if up else level]
        target = columns[-level - 1 if up else level + 1]
        rows = pl.ds(tile * tile_passages, tile_passages)
        return pltpu.make_async_remote_copy(
            src_ref=source.at[rows],
            dst_ref=target.at[rows],
            send_sem=hop_send.at[level, int(up), tile],
            recv_sem=hop_recv.at[level, int(up), tile],
            device_id=(me + plane if up else me - plane, tp),
            device_id_type=MESH,
        )

    def sends(level, up):
        if up:
            return (z >= level) & (z < depth - 1)
        return (z <= depth - 1 - level) & (z > 0)

    def gets(level, up):
        if up:
            return z >= level + 1
        return z <= depth - 2 - level

    def start_hop(level, tile):
        for up in (True, False):

            @pl.when(sends(level, up))
            def _(up=up):
                hop(level, up, tile).start()

    def await_hop(level, tile):
        for up in (True, False):

            @pl.when(gets(level, up))
            def _(up=up):
                hop(level, up, tile).wait_recv()

    def end_hop(level, tile):
        for up in (True, False):

            @pl.when(sends(level, up))
            def _(up=up):
                hop(level, up, tile).wait_send()

    loads[0].wait()
    loads[1].wait()

    @pl.loop(0, tiles)
    def _(tile):
        store_copy(tile).wait()
        normed = row_norm(store_buf[tile], passage_gain_ref[...])
        keys = head_norm(dot32(normed, key_w[...]), key_gain_ref[...])
        values = dot32(normed, value_w[...]).astype(jnp.bfloat16)
        rows = pl.ds(tile * tile_passages, tile_passages)
        columns[0][rows, :, :width] = keys.reshape(tile_passages, passage_len, width)
        columns[0][rows, :, width:] = values.reshape(tile_passages, passage_len, width)
        start_hop(0, tile)

    def take_ids(st):
        ids_arrival(st).wait_recv()
        ids_local(st).start()

    for_askers(take_ids)
    for_askers(lambda st: ids_local(st).wait())

    def plane_copy(offset, step):
        return pltpu.make_async_remote_copy(
            src_ref=picked.at[offset + REACH, step - 1],
            dst_ref=slots.at[z + offset, step],
            send_sem=plane_send.at[offset + REACH, step],
            recv_sem=plane_recv.at[offset + REACH, step],
            device_id=(z * plane + reader_place(step), tp),
            device_id_type=MESH,
        )

    def held(offset):
        return (z + offset >= 0) & (z + offset < depth)

    def deliver(offset):
        @pl.when(held(offset))
        def _():
            owner = (z + offset) * plane + p
            for step in range(plane - 1, -1, -1):
                reader = z * plane + reader_place(step)
                for rank in range(most):
                    entry = owner * most + rank
                    if step == 0:
                        index = wanted_smem[entry]
                        slots[z + offset, 0, rank] = columns[offset][index]
                    else:
                        index = ids_smem[reader, 0, entry]
                        picked[offset + REACH, step - 1, rank] = columns[offset][index]
            for step in range(plane - 1, 0, -1):
                plane_copy(offset, step).start()

    def far_row(other):
        near = jnp.minimum(z, REACH) + REACH + 1
        return jnp.where(other < z, other, jnp.maximum(other - near, 0))

    def far_copy(other, place):
        step = p ^ place if power else (place - p + plane) % plane
        return pltpu.make_async_remote_copy(
            src_ref=far_picked.at[far_row(other), place],
            dst_ref=slots.at[z, step],
            send_sem=far_send.at[other, place],
            recv_sem=far_recv.at[z, step],
            device_id=(other * plane + place, tp),
            device_id_type=MESH,
        )

    def far_arrival(other, step):
        return pltpu.make_async_remote_copy(
            src_ref=far_picked.at[far_row(other), step],
            dst_ref=slots.at[other, step],
            send_sem=far_send.at[other, step],
            recv_sem=far_recv.at[other, step],
            device_id=(other * plane + asker_place(step), tp),
            device_id_type=MESH,
        )

    def deliver_far():
        for other in far_planes:

            @pl.when(is_far(other))
            def _(other=other):
                for place in range(plane):
                    for rank in range(most):
                        index = ids_smem[other * plane + place, 0, me * most + rank]
                        far_picked[far_row(other), place, rank] = columns[0][index]
                for place in range(plane):
                    far_copy(other, place).start()

    deliver(0)

    for load in loads[2:5]:
        load.wait()
    x_copy.wait()
    swap.wait()
    taps = taps_ref.shape[0]
    lead = -(-(taps - 1) // 8) * 8
    length = tokens // SEQS_DEV
    channels = padded.shape[2]
    token_tile = min(256, length)
    per_sequence = length // token_tile
    for sequence in range(SEQS_DEV):
        padded[sequence, :lead, :] = jnp.zeros((lead, channels), jnp.float32)
        padded[sequence, lead + length :, :] = jnp.zeros((8, channels), jnp.float32)

    def project(tile):
        rows = pl.ds(pl.multiple_of(tile * token_tile, token_tile), token_tile)
        normed = row_norm(x_buf[rows, :], norm_gain_ref[...])
        queries[rows, :] = head_norm(dot32(normed, query_w[...]), query_gain_ref[...])
        value = dot32(normed, conv_value[...])
        gate = dot32(normed, conv_gate[...])
        gated = (value * jax.nn.sigmoid(gate)).astype(jnp.bfloat16).astype(jnp.float32)
        sequence, part = tile // per_sequence, tile % per_sequence
        start = pl.multiple_of(lead + part * token_tile, 8)
        padded[sequence, pl.ds(start, token_tile), :] = gated

    token_tiles = tokens // token_tile

    @pl.loop(0, token_tiles)
    def _(tile):
        project(tile)

        @pl.when(tile < tiles - 1)
        def _():
            await_hop(0, tile)
            start_hop(1, tile)

    chunk = 64
    span = chunk + lead + 8
    block_width = 256 if channels % 256 == 0 else channels

    def convolve(sequence):
        @pl.loop(0, length // chunk)
        def _(index):
            base = pl.multiple_of(index * chunk, chunk)
            for left in range(0, channels, block_width):
                cols = slice(left, left + block_width)
                window = padded[sequence, pl.ds(base, span), cols]
                total = jnp.zeros((chunk, block_width), jnp.float32)
                for shift in range(8):
                    moved = window if shift == 0 else pltpu.roll(window, span - shift, 0)
                    for start in range(0, lead + 1, 8):
                        tap = start + shift - (lead - taps + 1)
                        if 0 <= tap < taps:
                            weight = taps_ref[tap : tap + 1, cols].astype(jnp.float32)
                            total += weight * moved[start : start + chunk, :]
                out_rows = pl.ds(pl.multiple_of(sequence * length + base, chunk), chunk)
                filtered[out_rows, cols] = total

    convolve(0)
    for tile in range(min(token_tiles, tiles - 1), tiles):
        await_hop(0, tile)
        start_hop(1, tile)
    for distance in range(1, 2):
        deliver(-distance)
        deliver(distance)
    deliver_far()
    for sequence in range(1, SEQS_DEV):
        convolve(sequence)

    row_tile = 128

    @pl.loop(0, tokens // row_tile)
    def _(tile):
        rows = pl.ds(pl.multiple_of(tile * row_tile, row_tile), row_tile)
        block = filtered[rows, :]
        lane = lax.broadcasted_iota(jnp.int32, (row_tile, 128), 1)
        first = jnp.sum(block, axis=-1, keepdims=True)
        second = jnp.sum(block * block, axis=-1, keepdims=True)
        stats[rows, :] = jnp.where(lane == 0, first, second)

    def tp_copy(number, source, target):
        return pltpu.make_async_remote_copy(
            src_ref=source,
            dst_ref=target,
            send_sem=tp_send.at[number],
            recv_sem=tp_recv.at[number],
            device_id=(me, 1 - tp),
            device_id_type=MESH,
        )

    stats_copy = tp_copy(1, stats, stats_in)
    stats_copy.start()
    loads[5].wait()
    loads[6].wait()
    stats_copy.wait()

    @pl.loop(0, tokens // row_tile)
    def _(tile):
        rows = pl.ds(pl.multiple_of(tile * row_tile, row_tile), row_tile)
        sums = stats[rows, :] + stats_in[rows, :]
        mean = sums[:, 0:1] / C_A
        variance = sums[:, 1:2] / C_A - mean * mean
        scaled = (
            (filtered[rows, :] - mean)
            * lax.rsqrt(variance + LAYER_EPS)
            * ln_gain_ref[...].astype(jnp.float32)
        )
        acc[rows, :] = dot32(jax.nn.silu(scaled).astype(jnp.bfloat16), conv_out_w[...])

    for tile in range(tiles):
        await_hop(1, tile)
    for distance in range(2, REACH + 1):
        deliver(-distance)
        deliver(distance)
    for offset in OFFSETS:

        @pl.when(held(offset))
        def _(offset=offset):
            for step in range(1, plane):
                plane_copy(offset, step).wait_recv()

    for other in far_planes:

        @pl.when(is_far(other))
        def _(other=other):
            for step in range(plane):
                far_arrival(other, step).wait_recv()

    heads = width // MEM_HD
    blocks = slots_ref.shape[0] // passes
    block = tokens // blocks
    head_of = lax.broadcasted_iota(jnp.int32, (heads * block, width), 1) // MEM_HD
    row_head = lax.broadcasted_iota(jnp.int32, (heads * block, width), 0) // block
    inside = head_of == row_head
    gate = jnp.tanh(gate_ref[...].astype(jnp.float32))

    def attend(first, count):
        @pl.loop(0, count, unroll=4 if count % 4 == 0 else 1)
        def _(number):
            index = first + number
            rows = pl.ds(pl.multiple_of(index * block, block), block)
            query = queries[rows, :]
            stacked = jnp.concatenate([query] * heads, axis=0)
            stacked = jnp.where(inside, stacked, jnp.zeros_like(stacked))
            read = []
            for part in range(passes):
                slot = slots_ref[index * passes + part]
                read.append(slots[slot // (plane * most), slot // most % plane, slot % most])
            keys = jnp.concatenate([part[:, :width] for part in read], axis=0)
            values = jnp.concatenate([part[:, width:] for part in read], axis=0)
            scores = lax.dot_general(
                stacked, keys, (((1,), (1,)), ((), ())), preferred_element_type=jnp.float32
            ) * MEM_HD ** (-0.5)
            expanded = jnp.exp(scores - jnp.max(scores, axis=-1, keepdims=True))
            weights = (expanded / jnp.sum(expanded, axis=-1, keepdims=True)).astype(jnp.bfloat16)
            mixed = jnp.where(inside, dot32(weights, values), 0.0)
            attended = mixed[:block]
            for head in range(1, heads):
                attended = attended + mixed[head * block : (head + 1) * block]
            memory[rows, :] = (attended * gate).astype(jnp.bfloat16)

    share = tokens // 2
    pieces = part_out.shape[0]
    piece = share // pieces
    theirs, ours = (1 - tp) * share, tp * share
    attend((1 - tp) * (blocks // 2), blocks // 2)
    part_copies = [tp_copy(2 + n, part_out.at[n], part_in.at[n]) for n in range(pieces)]
    for number in range(pieces):
        rows = pl.ds(pl.multiple_of(theirs + number * piece, piece), piece)
        part_out[number] = (acc[rows, :] + dot32(memory[rows, :], mem_out_w[...])).astype(
            jnp.bfloat16
        )
        part_copies[number].start()
    attend(tp * (blocks // 2), blocks // 2)
    out_copies = [
        pltpu.make_async_copy(
            result.at[n], out_hbm.at[pl.ds(n * piece, piece)], out_sem.at[n]
        )
        for n in range(pieces)
    ]
    for number in range(pieces):
        rows = pl.ds(pl.multiple_of(ours + number * piece, piece), piece)
        kept = (acc[rows, :] + dot32(memory[rows, :], mem_out_w[...])).astype(jnp.bfloat16)
        part_copies[number].wait()
        result[number] = (
            kept.astype(jnp.float32) + part_in[number].astype(jnp.float32)
        ).astype(jnp.bfloat16)
        out_copies[number].start()

    for_askers(lambda st: ids_copy(st, st).wait_send())
    for level in range(REACH):
        for tile in range(tiles):
            end_hop(level, tile)
    for offset in OFFSETS:

        @pl.when(held(offset))
        def _(offset=offset):
            for step in range(1, plane):
                plane_copy(offset, step).wait_send()

    for other in far_planes:

        @pl.when(is_far(other))
        def _(other=other):
            for place in range(plane):
                far_copy(other, place).wait_send()

    for copy in out_copies:
        copy.wait()


def layer(
    tokens,
    passage_ids,
    passage_store,
    norm_gain,
    conv_value_weight,
    conv_gate_weight,
    conv_weight,
    ln_gain,
    query_weight,
    query_gain,
    passage_gain,
    key_weight,
    value_weight,
    key_gain,
    memory_gate,
    conv_out_weight,
    memory_out_weight,
):
    owner_count = lax.axis_size("st")
    me = lax.axis_index("st").astype(jnp.int32)
    depth, plane = split_axis(owner_count)
    power = plane & (plane - 1) == 0
    store_size, passage_len, features = passage_store.shape
    count, _ = tokens.shape
    width = key_weight.shape[1]
    channels = conv_weight.shape[1]

    flat_ids = passage_ids.reshape(-1)
    request_count = flat_ids.shape[0]
    most = max(1, 2 * request_count // owner_count)
    owner_index = flat_ids // store_size
    local_index = flat_ids % store_size
    same = (owner_index[:, None] == owner_index[None, :]) & (
        jnp.arange(request_count)[:, None] > jnp.arange(request_count)[None, :]
    )
    rank = jnp.sum(same.astype(jnp.int32), axis=1)
    place, my_place = owner_index % plane, me % plane
    step_to = (place ^ my_place) if power else (my_place - place + plane) % plane
    slot_index = ((owner_index // plane) * plane + step_to) * most + rank
    entry = owner_index * most + rank
    wide = -(-owner_count * most // 128) * 128
    onehot = (entry[:, None] == jnp.arange(wide, dtype=jnp.int32)[None, :]).astype(jnp.int32)
    wanted = jnp.sum(onehot * local_index[:, None], axis=0)

    tile_passages = max(1, min(256 // passage_len, store_size))
    tiles = store_size // tile_passages
    lead = -(-(conv_weight.shape[0] - 1) // 8) * 8
    length = count // SEQS_DEV
    share = count // 2
    pieces = 2
    row = (passage_len, 2 * width)
    bf16, f32 = jnp.bfloat16, jnp.float32
    vmem = pl.BlockSpec(memory_space=pltpu.VMEM)
    smem = pl.BlockSpec(memory_space=pltpu.SMEM)
    anywhere = pl.BlockSpec(memory_space=pl.ANY)
    dma = pltpu.SemaphoreType.DMA
    weights = (
        key_weight,
        value_weight,
        query_weight,
        conv_value_weight,
        conv_gate_weight,
        conv_out_weight,
        memory_out_weight,
    )
    reach = len(OFFSETS)
    scratch = (
        [pltpu.VMEM(w.shape, bf16) for w in weights]
        + [
            pltpu.VMEM((tiles, tile_passages * passage_len, features), bf16),
            pltpu.VMEM((count, features), bf16),
            pltpu.VMEM((SEQS_DEV, lead + length + 8, channels), f32),
            pltpu.VMEM((count, channels), f32),
            pltpu.VMEM((count, features), f32),
            pltpu.VMEM((count, width), bf16),
            pltpu.VMEM((count, width), bf16),
            pltpu.VMEM((count, 128), f32),
            pltpu.VMEM((count, 128), f32),
            pltpu.VMEM((pieces, share // pieces, features), bf16),
            pltpu.VMEM((pieces, share // pieces, features), bf16),
            pltpu.VMEM((pieces, share // pieces, features), bf16),
            pltpu.VMEM((owner_count, 1, wide), jnp.int32),
            pltpu.SMEM((owner_count, 1, wide), jnp.int32),
            pltpu.VMEM((depth, plane, most) + row, bf16),
        ]
        + [pltpu.VMEM((store_size,) + row, bf16) for _ in OFFSETS]
        + [
            pltpu.VMEM((reach, max(plane - 1, 1), most) + row, bf16),
            pltpu.VMEM((max(depth - 1 - REACH, 1), plane, most) + row, bf16),
            dma((len(weights),)),
            dma((tiles,)),
            dma,
            dma((owner_count,)),
            dma((owner_count,)),
            dma((owner_count,)),
            dma((REACH, 2, tiles)),
            dma((REACH, 2, tiles)),
            dma((reach, plane)),
            dma((reach, plane)),
            dma((depth, plane)),
            dma((depth, plane)),
            dma((2 + pieces,)),
            dma((2 + pieces,)),
            dma((pieces,)),
        ]
    )
    return pl.pallas_call(
        functools.partial(layer_kernel, depth, plane, most, passage_ids.shape[1]),
        in_specs=[smem, smem] + [vmem] * 8 + [anywhere] * (2 + len(weights)),
        out_specs=anywhere,
        out_shape=jax.ShapeDtypeStruct((share, features), bf16),
        scratch_shapes=scratch,
        compiler_params=pltpu.CompilerParams(
            collective_id=0, has_side_effects=True, vmem_limit_bytes=67043328
        ),
        cost_estimate=pl.CostEstimate(
            flops=16 << 30, bytes_accessed=24 << 20, transcendentals=0
        ),
        name="layer",
    )(
        slot_index,
        wanted,
        wanted[None, :],
        norm_gain[None, :],
        passage_gain[None, :],
        key_gain[None, :],
        query_gain[None, :],
        ln_gain[None, :],
        memory_gate[None, :],
        conv_weight,
        tokens,
        passage_store.reshape(-1, features),
        *weights,
    )


def solution(mesh):
    return jax.shard_map(
        layer,
        mesh=mesh,
        in_specs=(
            P("st", "tp"),
            P("st", None),
            P("st", None, None),
            P(),
            P(None, "tp"),
            P(None, "tp"),
            P(None, "tp"),
            P("tp"),
            P(None, "tp"),
            P("tp"),
            P(),
            P(None, "tp"),
            P(None, "tp"),
            P("tp"),
            P("tp"),
            P("tp", None),
            P("tp", None),
        ),
        out_specs=P(("st", "tp"), None),
        check_vma=False,
    )
```

profile of v0, /device:TPU:0, one launch (start us, length us, event | category | flops | bytes accessed | tf_op | source)
XLA Modules:
  0.0 110.8 jit_solution(15824776743668266296)
XLA Ops:
  0.0 1.2 %broadcast_in_dim.32.query_gain_ref = bf16[1,256]{1,0:T(2,128)(2,1)} reshape(bf16[256]{0:T(256)(128)(2,1)} %param.26) | data formatting | bytes 1024 | tf_op jit(solution)/shard_map/broadcast_in_dim | solution.py:719
  1.2 1.2 %broadcast_in_dim.31.key_gain_ref = bf16[1,256]{1,0:T(2,128)(2,1)} reshape(bf16[256]{0:T(256)(128)(2,1)} %param.30) | data formatting | bytes 1024 | tf_op jit(solution)/shard_map/broadcast_in_dim | solution.py:718
  2.4 1.2 %broadcast_in_dim.34.gate_ref = bf16[1,256]{1,0:T(2,128)(2,1)} reshape(bf16[256]{0:T(256)(128)(2,1)} %param.31) | data formatting | bytes 1024 | tf_op jit(solution)/shard_map/broadcast_in_dim | solution.py:721
  3.7 1.3 %broadcast_in_dim.33.ln_gain_ref = bf16[1,768]{1,0:T(2,128)(2,1)} reshape(bf16[768]{0:T(1024)(128)(2,1)} %param.24) | data formatting | bytes 3072 | tf_op jit(solution)/shard_map/broadcast_in_dim | solution.py:720
  4.9 0.8 copy.20
  5.7 0.1 reshape.96
  5.8 0.2 convert_reduce_fusion
  6.0 0.5 multiply_add_fusion
  6.5 0.6 select_reduce_fusion.wanted_smem
  7.1 1.3 %broadcast_in_dim.29.norm_gain_ref = bf16[1,2048]{1,0:T(2,128)(2,1)} reshape(bf16[2048]{0:T(1024)(128)(2,1)} %param.20) | data formatting | bytes 8192 | tf_op jit(solution)/shard_map/broadcast_in_dim | solution.py:716
  8.4 1.3 %broadcast_in_dim.30.passage_gain_ref = bf16[1,2048]{1,0:T(2,128)(2,1)} reshape(bf16[2048]{0:T(1024)(128)(2,1)} %param.27) | data formatting | bytes 8192 | tf_op jit(solution)/shard_map/broadcast_in_dim | solution.py:717
  9.7 97.9 %layer.1 = bf16[512,2048]{1,0:T(8,128)(2,1)} custom-call(s32[32]{0:T(128)} %get-tuple-element.6.slots_ref, s32[128]{0:T(128)} %select_reduce_fusion.wanted_smem, s32[1,128]{1,0:T(1,128)} %bitcast.3, bf16[1,2048]{1,0:T(2,128)(2,1)} %broadcast_in_dim.29.norm_gain_ref, bf16[1,2048]{1,0:T(2,128)(2,1)} %broadcast_in_dim.30.passage_gain_ref, ...), custom_call_target="tpu_custom_call" | custom-call | flops 17179869184 | bytes 25165824 | tf_op jit(solution)/shard_map/layer/pallas_call | solution.py:699
  107.6 3.2 %copy.22 = bf16[512,2048]{1,0:T(8,128)(2,1)} copy(bf16[512,2048]{1,0:T(8,128)(2,1)} %layer.1) | data formatting | bytes 4194304
  (1 shorter events, 0.0 us)
where the time goes:
time: 111 us
  Pallas kernels  97.9 us (88%)
  local copies, waits for them, and re-layouts  11.5 us (10%)
  other arithmetic  1.33 us (1%)
    pallas_call x1, Pallas kernels, layer(): pl.pallas_call(functools.partial(layer_kernel, depth, plane, most, passag...  97.9 us
    unnamed x2, local copies, waits for them, and re-layouts  3.91 us

commit v1 on v0

--- a/solution.py
+++ b/solution.py
@@ -25,7 +25,7 @@
         inside = (lane >= head * MEM_HD) & (lane < (head + 1) * MEM_HD)
         total = jnp.sum(jnp.where(inside, squares, 0.0), axis=-1, keepdims=True)
         scale = jnp.where(inside, lax.rsqrt(total * (1.0 / MEM_HD) + NORM_EPS), scale)
-    return (product * scale * gain_row.astype(jnp.float32)).astype(jnp.bfloat16)
+    return (product * scale * gain_row).astype(jnp.bfloat16)
 
 
 def dot32(left, right):
@@ -35,7 +35,7 @@
 def row_norm(rows, gain_row):
     wide = rows.astype(jnp.float32)
     factor = lax.rsqrt(jnp.mean(wide * wide, axis=-1, keepdims=True) + NORM_EPS)
-    return (wide * factor * gain_row.astype(jnp.float32)).astype(jnp.bfloat16)
+    return (wide * factor * gain_row).astype(jnp.bfloat16)
 
 
 def split_axis(count):
@@ -70,7 +70,8 @@
     conv_gate_hbm,
     conv_out_hbm,
     mem_out_hbm,
-    out_hbm,
+    keep_hbm,
+    back_hbm,
     key_w,
     value_w,
     query_w,
@@ -88,8 +89,7 @@
     stats,
     stats_in,
     part_out,
-    part_in,
-    result,
+    part_keep,
     ids_in,
     ids_smem,
     slots,
@@ -294,8 +294,8 @@
     @pl.loop(0, tiles)
     def _(tile):
         store_copy(tile).wait()
-        normed = row_norm(store_buf[tile], passage_gain_ref[...])
-        keys = head_norm(dot32(normed, key_w[...]), key_gain_ref[...])
+        normed = row_norm(store_buf[tile], passage_gain_ref[...].astype(jnp.float32)[None, :])
+        keys = head_norm(dot32(normed, key_w[...]), key_gain_ref[...].astype(jnp.float32)[None, :])
         values = dot32(normed, value_w[...]).astype(jnp.bfloat16)
         rows = pl.ds(tile * tile_passages, tile_passages)
         columns[0][rows, :, :width] = keys.reshape(tile_passages, passage_len, width)
@@ -394,8 +394,8 @@
 
     def project(tile):
         rows = pl.ds(pl.multiple_of(tile * token_tile, token_tile), token_tile)
-        normed = row_norm(x_buf[rows, :], norm_gain_ref[...])
-        queries[rows, :] = head_norm(dot32(normed, query_w[...]), query_gain_ref[...])
+        normed = row_norm(x_buf[rows, :], norm_gain_ref[...].astype(jnp.float32)[None, :])
+        queries[rows, :] = head_norm(dot32(normed, query_w[...]), query_gain_ref[...].astype(jnp.float32)[None, :])
         value = dot32(normed, conv_value[...])
         gate = dot32(normed, conv_gate[...])
         gated = (value * jax.nn.sigmoid(gate)).astype(jnp.bfloat16).astype(jnp.float32)
@@ -443,7 +443,6 @@
     for distance in range(1, 2):
         deliver(-distance)
         deliver(distance)
-    deliver_far()
     for sequence in range(1, SEQS_DEV):
         convolve(sequence)
 
@@ -483,7 +482,7 @@
         scaled = (
             (filtered[rows, :] - mean)
             * lax.rsqrt(variance + LAYER_EPS)
-            * ln_gain_ref[...].astype(jnp.float32)
+            * ln_gain_ref[...].astype(jnp.float32)[None, :]
         )
         acc[rows, :] = dot32(jax.nn.silu(scaled).astype(jnp.bfloat16), conv_out_w[...])
 
@@ -492,6 +491,7 @@
     for distance in range(2, REACH + 1):
         deliver(-distance)
         deliver(distance)
+    deliver_far()
     for offset in OFFSETS:
 
         @pl.when(held(offset))
@@ -512,7 +512,7 @@
     head_of = lax.broadcasted_iota(jnp.int32, (heads * block, width), 1) // MEM_HD
     row_head = lax.broadcasted_iota(jnp.int32, (heads * block, width), 0) // block
     inside = head_of == row_head
-    gate = jnp.tanh(gate_ref[...].astype(jnp.float32))
+    gate = jnp.tanh(gate_ref[...].astype(jnp.float32)[None, :])
 
     def attend(first, count):
         @pl.loop(0, count, unroll=4 if count % 4 == 0 else 1)
@@ -544,7 +544,10 @@
     piece = share // pieces
     theirs, ours = (1 - tp) * share, tp * share
     attend((1 - tp) * (blocks // 2), blocks // 2)
-    part_copies = [tp_copy(2 + n, part_out.at[n], part_in.at[n]) for n in range(pieces)]
+    part_copies = [
+        tp_copy(2 + n, part_out.at[n], back_hbm.at[pl.ds(n * piece, piece)])
+        for n in range(pieces)
+    ]
     for number in range(pieces):
         rows = pl.ds(pl.multiple_of(theirs + number * piece, piece), piece)
         part_out[number] = (acc[rows, :] + dot32(memory[rows, :], mem_out_w[...])).astype(
@@ -554,17 +557,15 @@
     attend(tp * (blocks // 2), blocks // 2)
     out_copies = [
         pltpu.make_async_copy(
-            result.at[n], out_hbm.at[pl.ds(n * piece, piece)], out_sem.at[n]
+            part_keep.at[n], keep_hbm.at[pl.ds(n * piece, piece)], out_sem.at[n]
         )
         for n in range(pieces)
     ]
     for number in range(pieces):
         rows = pl.ds(pl.multiple_of(ours + number * piece, piece), piece)
-        kept = (acc[rows, :] + dot32(memory[rows, :], mem_out_w[...])).astype(jnp.bfloat16)
-        part_copies[number].wait()
-        result[number] = (
-            kept.astype(jnp.float32) + part_in[number].astype(jnp.float32)
-        ).astype(jnp.bfloat16)
+        part_keep[number] = (acc[rows, :] + dot32(memory[rows, :], mem_out_w[...])).astype(
+            jnp.bfloat16
+        )
         out_copies[number].start()
 
     for_askers(lambda st: ids_copy(st, st).wait_send())
@@ -585,8 +586,29 @@
             for place in range(plane):
                 far_copy(other, place).wait_send()
 
-    for copy in out_copies:
+    for copy in part_copies + out_copies:
         copy.wait()
+
+
+def add_kernel(keep_ref, back_ref, out_ref):
+    out_ref[...] = (
+        keep_ref[...].astype(jnp.float32) + back_ref[...].astype(jnp.float32)
+    ).astype(jnp.bfloat16)
+
+
+def add_parts(keep, back):
+    rows, features = keep.shape
+    tile = min(128, rows)
+    spec = pl.BlockSpec((tile, features), lambda i: (i, 0))
+    return pl.pallas_call(
+        add_kernel,
+        grid=(rows // tile,),
+        in_specs=[spec, spec],
+        out_specs=spec,
+        out_shape=jax.ShapeDtypeStruct(keep.shape, jnp.bfloat16),
+        compiler_params=pltpu.CompilerParams(dimension_semantics=("arbitrary",)),
+        name="add_parts",
+    )(keep, back)
 
 
 def layer(
@@ -670,7 +692,6 @@
             pltpu.VMEM((count, 128), f32),
             pltpu.VMEM((pieces, share // pieces, features), bf16),
             pltpu.VMEM((pieces, share // pieces, features), bf16),
-            pltpu.VMEM((pieces, share // pieces, features), bf16),
             pltpu.VMEM((owner_count, 1, wide), jnp.int32),
             pltpu.SMEM((owner_count, 1, wide), jnp.int32),
             pltpu.VMEM((depth, plane, most) + row, bf16),
@@ -696,11 +717,11 @@
             dma((pieces,)),
         ]
     )
-    return pl.pallas_call(
+    keep, back = pl.pallas_call(
         functools.partial(layer_kernel, depth, plane, most, passage_ids.shape[1]),
         in_specs=[smem, smem] + [vmem] * 8 + [anywhere] * (2 + len(weights)),
-        out_specs=anywhere,
-        out_shape=jax.ShapeDtypeStruct((share, features), bf16),
+        out_specs=[anywhere] * 2,
+        out_shape=[jax.ShapeDtypeStruct((share, features), bf16)] * 2,
         scratch_shapes=scratch,
         compiler_params=pltpu.CompilerParams(
             collective_id=0, has_side_effects=True, vmem_limit_bytes=67043328
@@ -713,17 +734,18 @@
         slot_index,
         wanted,
         wanted[None, :],
-        norm_gain[None, :],
-        passage_gain[None, :],
-        key_gain[None, :],
-        query_gain[None, :],
-        ln_gain[None, :],
-        memory_gate[None, :],
+        norm_gain,
+        passage_gain,
+        key_gain,
+        query_gain,
+        ln_gain,
+        memory_gate,
         conv_weight,
         tokens,
         passage_store.reshape(-1, features),
         *weights,
     )
+    return add_parts(keep, back)
 
 
 def solution(mesh):

time: 111 us -> 97.8 us (0.88)
  the two profiles are of different devices: /device:TPU:0 before, /device:TPU:6 now
where the time goes in v1:
time: 97.8 us; the launch traced here: 97.6 us
  Pallas kernels  95.4 us (98%)
  other arithmetic  1.33 us (1%)
    pallas_call x1, Pallas kernels, layer(): pl.pallas_call(functools.partial(layer_kernel, depth, plane, most, passag...  91 us
    pallas_call x1, Pallas kernels, add_parts(): pl.pallas_call(add_kernel, grid=(rows // tile,), in_specs=[spec, spec], o...  4.31 us

profile of v1, /device:TPU:6, one launch (start us, length us, event | category | flops | bytes accessed | tf_op | source)
XLA Modules:
  0.0 97.6 jit_solution(8080197873882535575)
XLA Ops:
  0.0 0.8 copy.20
  0.8 0.1 reshape.96
  0.9 0.2 convert_reduce_fusion
  1.0 0.5 multiply_add_fusion
  1.6 0.6 select_reduce_fusion.wanted_smem
  2.2 91.0 %layer.1 = (bf16[512,2048]{1,0:T(8,128)(2,1)}, bf16[512,2048]{1,0:T(8,128)(2,1)}) custom-call(s32[32]{0:T(128)} %get-tuple-element.10.slots_ref, s32[128]{0:T(128)} %select_reduce_fusion.wanted_smem, s32[1,128]{1,0:T(1,128)} %bitcast.3, bf16[2048]{0:T(1024)(128)(2,1)} %norm_gain_ref.1, bf16[2048]{0:T(1024)(128)(2,1)} %passage_gain_ref.1, ...), custom_call_target="tpu_custom_call" | custom-call | flops 17179869184 | bytes 25165824 | tf_op jit(solution)/shard_map/layer/pallas_call | solution.py:720
  93.2 4.3 %add_parts.1 = bf16[512,2048]{1,0:T(8,128)(2,1)} custom-call(bf16[512,2048]{1,0:T(8,128)(2,1)} %get-tuple-element.7.keep_ref, bf16[512,2048]{1,0:T(8,128)(2,1)} %get-tuple-element.8.back_ref), custom_call_target="tpu_custom_call" | custom-call | tf_op jit(solution)/shard_map/add_parts/pallas_call | solution.py:603
  (1 shorter events, 0.0 us)

commit v2 on v1

--- a/solution.py
+++ b/solution.py
@@ -51,9 +51,7 @@
     plane,
     most,
     passes,
-    slots_ref,
-    wanted_smem,
-    wanted_ref,
+    ids_ref,
     norm_gain_ref,
     passage_gain_ref,
     key_gain_ref,
@@ -70,8 +68,8 @@
     conv_gate_hbm,
     conv_out_hbm,
     mem_out_hbm,
-    keep_hbm,
-    back_hbm,
+    keep_ref,
+    back_ref,
     key_w,
     value_w,
     query_w,
@@ -88,8 +86,9 @@
     memory,
     stats,
     stats_in,
-    part_out,
-    part_keep,
+    wanted_ref,
+    wanted_smem,
+    slots_ref,
     ids_in,
     ids_smem,
     slots,
@@ -99,9 +98,11 @@
     (
         picked,
         far_picked,
+        far_stage,
         load_sem,
         store_sem,
         x_sem,
+        wanted_sem,
         ids_copy_sem,
         ids_send,
         ids_recv,
@@ -109,11 +110,12 @@
         hop_recv,
         plane_send,
         plane_recv,
+        stage_send,
+        stage_recv,
         far_send,
         far_recv,
         tp_send,
         tp_recv,
-        out_sem,
     ) = rest
     me = lax.axis_index("st")
     tp = lax.axis_index("tp")
@@ -131,9 +133,6 @@
     def reader_place(step):
         return p ^ step if power else (p + step) % plane
 
-    def asker_place(step):
-        return p ^ step if power else (p - step + plane) % plane
-
     far_planes = [o for o in range(depth) if max(o, depth - 1 - o) > REACH]
 
     def is_far(other):
@@ -165,38 +164,69 @@
     store_copy(0).start()
     loads[0].start()
     loads[1].start()
+    barrier = pltpu.get_barrier_semaphore()
+
+    def greet(st, core):
+        pl.semaphore_signal(barrier, inc=1, device_id=(st, core), device_id_type=MESH)
+
+    greet(me, 1 - tp)
+    for step in range(1, plane):
+        greet(z * plane + reader_place(step), tp)
+
+    @pl.when(z > 0)
+    def _():
+        greet(me - plane, tp)
+
+    @pl.when(z < depth - 1)
+    def _():
+        greet(me + plane, tp)
+
+    met = 1 + plane - 1 + jnp.where(z > 0, 1, 0) + jnp.where(z < depth - 1, 1, 0)
+    for other in far_planes:
+
+        @pl.when(is_far(other))
+        def _(other=other):
+            for place in range(plane):
+                greet(other * plane + place, tp)
+
+        met = met + jnp.where(is_far(other), plane, 0)
+
+    requests = slots_ref.shape[0]
+    owners, rows_asked = [], []
+    for number in range(requests):
+        asked = ids_ref[number % passes, number // passes]
+        owners.append(lax.div(asked, store_size))
+        rows_asked.append(lax.rem(asked, store_size))
+    lane = lax.broadcasted_iota(jnp.int32, wanted_ref.shape, 1)
+    wanted = jnp.zeros(wanted_ref.shape, jnp.int32)
+    for number, owner in enumerate(owners):
+        rank = jnp.int32(0)
+        for before in owners[:number]:
+            rank = rank + (before == owner).astype(jnp.int32)
+        place = lax.rem(owner, plane)
+        step = place ^ p if power else lax.rem(p - place + plane, plane)
+        slots_ref[number] = (lax.div(owner, plane) * plane + step) * most + rank
+        wanted = wanted + jnp.where(lane == owner * most + rank, rows_asked[number], 0)
+    wanted_ref[...] = wanted
+    own_ids = pltpu.make_async_copy(wanted_ref, wanted_smem, wanted_sem)
+
+    def project_passages(tile):
+        normed = row_norm(store_buf[tile], passage_gain_ref[...].astype(jnp.float32)[None, :])
+        keys = head_norm(dot32(normed, key_w[...]), key_gain_ref[...].astype(jnp.float32)[None, :])
+        values = dot32(normed, value_w[...]).astype(jnp.bfloat16)
+        rows = pl.ds(tile * tile_passages, tile_passages)
+        columns[0][rows, :, :width] = keys.reshape(tile_passages, passage_len, width)
+        columns[0][rows, :, width:] = values.reshape(tile_passages, passage_len, width)
+
+    loads[0].wait()
+    loads[1].wait()
+    store_copy(0).wait()
     for tile in range(1, tiles):
         store_copy(tile).start()
     x_copy.start()
     for load in loads[2:]:
         load.start()
-
-    barrier = pltpu.get_barrier_semaphore()
-
-    def greet(st, core):
-        pl.semaphore_signal(barrier, inc=1, device_id=(st, core), device_id_type=MESH)
-
-    greet(me, 1 - tp)
-    for step in range(1, plane):
-        greet(z * plane + reader_place(step), tp)
-
-    @pl.when(z > 0)
-    def _():
-        greet(me - plane, tp)
-
-    @pl.when(z < depth - 1)
-    def _():
-        greet(me + plane, tp)
-
-    met = 1 + plane - 1 + jnp.where(z > 0, 1, 0) + jnp.where(z < depth - 1, 1, 0)
-    for other in far_planes:
-
-        @pl.when(is_far(other))
-        def _(other=other):
-            for place in range(plane):
-                greet(other * plane + place, tp)
-
-        met = met + jnp.where(is_far(other), plane, 0)
+    project_passages(0)
     pl.semaphore_wait(barrier, met)
 
     def ids_copy(st, send_slot):
@@ -231,18 +261,6 @@
             def _(other=other):
                 for place in range(plane):
                     action(other * plane + place)
-
-    for_askers(lambda st: ids_copy(st, st).start())
-
-    swap = pltpu.make_async_remote_copy(
-        src_ref=tokens_hbm,
-        dst_ref=x_buf.at[:, mine],
-        send_sem=tp_send.at[0],
-        recv_sem=tp_recv.at[0],
-        device_id=(me, 1 - tp),
-        device_id_type=MESH,
-    )
-    swap.start()
 
     def hop(level, up, tile):
         source = columns[-level if up else level]
@@ -288,18 +306,24 @@
             def _(up=up):
                 hop(level, up, tile).wait_send()
 
-    loads[0].wait()
-    loads[1].wait()
-
-    @pl.loop(0, tiles)
+    own_ids.start()
+    for_askers(lambda st: ids_copy(st, st).start())
+    start_hop(0, 0)
+
+    swap = pltpu.make_async_remote_copy(
+        src_ref=tokens_hbm,
+        dst_ref=x_buf.at[:, mine],
+        send_sem=tp_send.at[0],
+        recv_sem=tp_recv.at[0],
+        device_id=(me, 1 - tp),
+        device_id_type=MESH,
+    )
+    swap.start()
+
+    @pl.loop(1, tiles)
     def _(tile):
         store_copy(tile).wait()
-        normed = row_norm(store_buf[tile], passage_gain_ref[...].astype(jnp.float32)[None, :])
-        keys = head_norm(dot32(normed, key_w[...]), key_gain_ref[...].astype(jnp.float32)[None, :])
-        values = dot32(normed, value_w[...]).astype(jnp.bfloat16)
-        rows = pl.ds(tile * tile_passages, tile_passages)
-        columns[0][rows, :, :width] = keys.reshape(tile_passages, passage_len, width)
-        columns[0][rows, :, width:] = values.reshape(tile_passages, passage_len, width)
+        project_passages(tile)
         start_hop(0, tile)
 
     def take_ids(st):
@@ -308,6 +332,7 @@
 
     for_askers(take_ids)
     for_askers(lambda st: ids_local(st).wait())
+    own_ids.wait()
 
     def plane_copy(offset, step):
         return pltpu.make_async_remote_copy(
@@ -331,7 +356,7 @@
                 for rank in range(most):
                     entry = owner * most + rank
                     if step == 0:
-                        index = wanted_smem[entry]
+                        index = wanted_smem[0, entry]
                         slots[z + offset, 0, rank] = columns[offset][index]
                     else:
                         index = ids_smem[reader, 0, entry]
@@ -343,40 +368,52 @@
         near = jnp.minimum(z, REACH) + REACH + 1
         return jnp.where(other < z, other, jnp.maximum(other - near, 0))
 
-    def far_copy(other, place):
-        step = p ^ place if power else (place - p + plane) % plane
+    def stage_copy(other, step):
         return pltpu.make_async_remote_copy(
-            src_ref=far_picked.at[far_row(other), place],
-            dst_ref=slots.at[z, step],
-            send_sem=far_send.at[other, place],
-            recv_sem=far_recv.at[z, step],
-            device_id=(other * plane + place, tp),
+            src_ref=far_picked.at[far_row(other), step - 1],
+            dst_ref=far_stage.at[far_row(other), step],
+            send_sem=stage_send.at[far_row(other), step],
+            recv_sem=stage_recv.at[far_row(other), step],
+            device_id=(z * plane + reader_place(step), tp),
             device_id_type=MESH,
         )
 
-    def far_arrival(other, step):
+    def far_copy(other, source):
         return pltpu.make_async_remote_copy(
-            src_ref=far_picked.at[far_row(other), step],
-            dst_ref=slots.at[other, step],
-            send_sem=far_send.at[other, step],
-            recv_sem=far_recv.at[other, step],
-            device_id=(other * plane + asker_place(step), tp),
+            src_ref=far_stage.at[far_row(other)],
+            dst_ref=slots.at[source],
+            send_sem=far_send.at[other],
+            recv_sem=far_recv.at[source],
+            device_id=(other * plane + p, tp),
             device_id_type=MESH,
         )
 
-    def deliver_far():
+    def for_far(action):
         for other in far_planes:
 
             @pl.when(is_far(other))
             def _(other=other):
-                for place in range(plane):
-                    for rank in range(most):
-                        index = ids_smem[other * plane + place, 0, me * most + rank]
-                        far_picked[far_row(other), place, rank] = columns[0][index]
-                for place in range(plane):
-                    far_copy(other, place).start()
+                action(other)
+
+    def stage_far(other):
+        for step in range(plane - 1, -1, -1):
+            reader = other * plane + reader_place(step)
+            for rank in range(most):
+                block = columns[0][ids_smem[reader, 0, me * most + rank]]
+                if step == 0:
+                    far_stage[far_row(other), 0, rank] = block
+                else:
+                    far_picked[far_row(other), step - 1, rank] = block
+        for step in range(plane - 1, 0, -1):
+            stage_copy(other, step).start()
+
+    def send_far(other):
+        for step in range(1, plane):
+            stage_copy(other, step).wait_recv()
+        far_copy(other, z).start()
 
     deliver(0)
+    for_far(stage_far)
 
     for load in loads[2:5]:
         load.wait()
@@ -491,7 +528,7 @@
     for distance in range(2, REACH + 1):
         deliver(-distance)
         deliver(distance)
-    deliver_far()
+    for_far(send_far)
     for offset in OFFSETS:
 
         @pl.when(held(offset))
@@ -499,12 +536,7 @@
             for step in range(1, plane):
                 plane_copy(offset, step).wait_recv()
 
-    for other in far_planes:
-
-        @pl.when(is_far(other))
-        def _(other=other):
-            for step in range(plane):
-                far_arrival(other, step).wait_recv()
+    for_far(lambda other: far_copy(other, other).wait_recv())
 
     heads = width // MEM_HD
     blocks = slots_ref.shape[0] // passes
@@ -540,33 +572,26 @@
             memory[rows, :] = (attended * gate).astype(jnp.bfloat16)
 
     share = tokens // 2
-    pieces = part_out.shape[0]
-    piece = share // pieces
-    theirs, ours = (1 - tp) * share, tp * share
-    attend((1 - tp) * (blocks // 2), blocks // 2)
-    part_copies = [
-        tp_copy(2 + n, part_out.at[n], back_hbm.at[pl.ds(n * piece, piece)])
-        for n in range(pieces)
-    ]
-    for number in range(pieces):
-        rows = pl.ds(pl.multiple_of(theirs + number * piece, piece), piece)
-        part_out[number] = (acc[rows, :] + dot32(memory[rows, :], mem_out_w[...])).astype(
-            jnp.bfloat16
-        )
-        part_copies[number].start()
-    attend(tp * (blocks // 2), blocks // 2)
-    out_copies = [
-        pltpu.make_async_copy(
-            part_keep.at[n], keep_hbm.at[pl.ds(n * piece, piece)], out_sem.at[n]
-        )
-        for n in range(pieces)
-    ]
-    for number in range(pieces):
-        rows = pl.ds(pl.multiple_of(ours + number * piece, piece), piece)
-        part_keep[number] = (acc[rows, :] + dot32(memory[rows, :], mem_out_w[...])).astype(
-            jnp.bfloat16
-        )
-        out_copies[number].start()
+    pieces = tp_send.shape[0] - 2
+    piece, few = share // pieces, blocks // 2 // pieces
+
+    def part_copy(number):
+        rows = pl.ds(pl.multiple_of(number * piece, piece), piece)
+        return tp_copy(2 + number, x_buf.at[rows], back_ref.at[rows])
+
+    def part_of(core, number):
+        attend(core * (blocks // 2) + number * few, few)
+        rows = pl.ds(pl.multiple_of(core * share + number * piece, piece), piece)
+        return (acc[rows, :] + dot32(memory[rows, :], mem_out_w[...])).astype(jnp.bfloat16)
+
+    @pl.loop(0, pieces)
+    def _(number):
+        x_buf[pl.ds(pl.multiple_of(number * piece, piece), piece), :] = part_of(1 - tp, number)
+        part_copy(number).start()
+
+    @pl.loop(0, pieces)
+    def _(number):
+        keep_ref[pl.ds(pl.multiple_of(number * piece, piece), piece), :] = part_of(tp, number)
 
     for_askers(lambda st: ids_copy(st, st).wait_send())
     for level in range(REACH):
@@ -579,34 +604,46 @@
             for step in range(1, plane):
                 plane_copy(offset, step).wait_send()
 
-    for other in far_planes:
-
-        @pl.when(is_far(other))
-        def _(other=other):
-            for place in range(plane):
-                far_copy(other, place).wait_send()
-
-    for copy in part_copies + out_copies:
+    def end_far(other):
+        for step in range(1, plane):
+            stage_copy(other, step).wait_send()
+        far_copy(other, z).wait_send()
+
+    for_far(end_far)
+    for number in range(pieces):
+        part_copy(number).wait()
+
+
+def add_kernel(keep_ref, back_ref, out_hbm, result, sems):
+    pieces, piece = result.shape[:2]
+    copies = []
+    for number in range(pieces):
+        rows = pl.ds(number * piece, piece)
+        result[number] = (
+            keep_ref[rows, :].astype(jnp.float32) + back_ref[rows, :].astype(jnp.float32)
+        ).astype(jnp.bfloat16)
+        copies.append(
+            pltpu.make_async_copy(result.at[number], out_hbm.at[rows], sems.at[number])
+        )
+        copies[-1].start()
+    for copy in copies:
         copy.wait()
-
-
-def add_kernel(keep_ref, back_ref, out_ref):
-    out_ref[...] = (
-        keep_ref[...].astype(jnp.float32) + back_ref[...].astype(jnp.float32)
-    ).astype(jnp.bfloat16)
 
 
 def add_parts(keep, back):
     rows, features = keep.shape
-    tile = min(128, rows)
-    spec = pl.BlockSpec((tile, features), lambda i: (i, 0))
+    pieces = 4
+    vmem = pl.BlockSpec(memory_space=pltpu.VMEM)
     return pl.pallas_call(
         add_kernel,
-        grid=(rows // tile,),
-        in_specs=[spec, spec],
-        out_specs=spec,
+        in_specs=[vmem, vmem],
+        out_specs=pl.BlockSpec(memory_space=pl.ANY),
         out_shape=jax.ShapeDtypeStruct(keep.shape, jnp.bfloat16),
-        compiler_params=pltpu.CompilerParams(dimension_semantics=("arbitrary",)),
+        scratch_shapes=[
+            pltpu.VMEM((pieces, rows // pieces, features), jnp.bfloat16),
+            pltpu.SemaphoreType.DMA((pieces,)),
+        ],
+        compiler_params=pltpu.CompilerParams(vmem_limit_bytes=16 << 20),
         name="add_parts",
     )(keep, back)
 
@@ -631,30 +668,15 @@
     memory_out_weight,
 ):
     owner_count = lax.axis_size("st")
-    me = lax.axis_index("st").astype(jnp.int32)
     depth, plane = split_axis(owner_count)
-    power = plane & (plane - 1) == 0
     store_size, passage_len, features = passage_store.shape
     count, _ = tokens.shape
     width = key_weight.shape[1]
     channels = conv_weight.shape[1]
 
-    flat_ids = passage_ids.reshape(-1)
-    request_count = flat_ids.shape[0]
+    request_count = passage_ids.shape[0] * passage_ids.shape[1]
     most = max(1, 2 * request_count // owner_count)
-    owner_index = flat_ids // store_size
-    local_index = flat_ids % store_size
-    same = (owner_index[:, None] == owner_index[None, :]) & (
-        jnp.arange(request_count)[:, None] > jnp.arange(request_count)[None, :]
-    )
-    rank = jnp.sum(same.astype(jnp.int32), axis=1)
-    place, my_place = owner_index % plane, me % plane
-    step_to = (place ^ my_place) if power else (my_place - place + plane) % plane
-    slot_index = ((owner_index // plane) * plane + step_to) * most + rank
-    entry = owner_index * most + rank
     wide = -(-owner_count * most // 128) * 128
-    onehot = (entry[:, None] == jnp.arange(wide, dtype=jnp.int32)[None, :]).astype(jnp.int32)
-    wanted = jnp.sum(onehot * local_index[:, None], axis=0)
 
     tile_passages = max(1, min(256 // passage_len, store_size))
     tiles = store_size // tile_passages
@@ -678,6 +700,7 @@
         memory_out_weight,
     )
     reach = len(OFFSETS)
+    far_rows = max(depth - 1 - REACH, 1)
     scratch = (
         [pltpu.VMEM(w.shape, bf16) for w in weights]
         + [
@@ -690,8 +713,9 @@
             pltpu.VMEM((count, width), bf16),
             pltpu.VMEM((count, 128), f32),
             pltpu.VMEM((count, 128), f32),
-            pltpu.VMEM((pieces, share // pieces, features), bf16),
-            pltpu.VMEM((pieces, share // pieces, features), bf16),
+            pltpu.VMEM((1, wide), jnp.int32),
+            pltpu.SMEM((1, wide), jnp.int32),
+            pltpu.SMEM((request_count,), jnp.int32),
             pltpu.VMEM((owner_count, 1, wide), jnp.int32),
             pltpu.SMEM((owner_count, 1, wide), jnp.int32),
             pltpu.VMEM((depth, plane, most) + row, bf16),
@@ -699,9 +723,11 @@
         + [pltpu.VMEM((store_size,) + row, bf16) for _ in OFFSETS]
         + [
             pltpu.VMEM((reach, max(plane - 1, 1), most) + row, bf16),
-            pltpu.VMEM((max(depth - 1 - REACH, 1), plane, most) + row, bf16),
+            pltpu.VMEM((far_rows, max(plane - 1, 1), most) + row, bf16),
+            pltpu.VMEM((far_rows, plane, most) + row, bf16),
             dma((len(weights),)),
             dma((tiles,)),
+            dma,
             dma,
             dma((owner_count,)),
             dma((owner_count,)),
@@ -710,30 +736,29 @@
             dma((REACH, 2, tiles)),
             dma((reach, plane)),
             dma((reach, plane)),
-            dma((depth, plane)),
-            dma((depth, plane)),
+            dma((far_rows, plane)),
+            dma((far_rows, plane)),
+            dma((depth,)),
+            dma((depth,)),
             dma((2 + pieces,)),
             dma((2 + pieces,)),
-            dma((pieces,)),
         ]
     )
     keep, back = pl.pallas_call(
         functools.partial(layer_kernel, depth, plane, most, passage_ids.shape[1]),
-        in_specs=[smem, smem] + [vmem] * 8 + [anywhere] * (2 + len(weights)),
-        out_specs=[anywhere] * 2,
-        out_shape=[jax.ShapeDtypeStruct((share, features), bf16)] * 2,
+        in_specs=[smem] + [vmem] * 7 + [anywhere] * (2 + len(weights)),
+        out_specs=[vmem] * 2,
+        out_shape=[pltpu.VMEM((share, features), bf16)] * 2,
         scratch_shapes=scratch,
         compiler_params=pltpu.CompilerParams(
-            collective_id=0, has_side_effects=True, vmem_limit_bytes=67043328
+            collective_id=0, has_side_effects=True, vmem_limit_bytes=58 << 20
         ),
         cost_estimate=pl.CostEstimate(
             flops=16 << 30, bytes_accessed=24 << 20, transcendentals=0
         ),
         name="layer",
     )(
-        slot_index,
-        wanted,
-        wanted[None, :],
+        passage_ids.T,
         norm_gain,
         passage_gain,
         key_gain,

time: 97.8 us -> 87.4 us (0.89)
  the two profiles are of different devices: /device:TPU:6 before, /device:TPU:0 now
where the time goes in v2:
time: 87.4 us; the launch traced here: 87.3 us
  Pallas kernels  87.2 us (100%)
    pallas_call x1, Pallas kernels, layer(): pl.pallas_call(functools.partial(layer_kernel, depth, plane, most, passag...  85.8 us

profile of v2, /device:TPU:0, one launch (start us, length us, event | category | flops | bytes accessed | tf_op | source)
XLA Modules:
  0.0 87.3 jit_solution(16376041021747071075)
XLA Ops:
  0.0 85.8 %layer.1 = (bf16[512,2048]{1,0:T(8,128)(2,1)S(1)}, bf16[512,2048]{1,0:T(8,128)(2,1)S(1)}) custom-call(s32[2,16]{1,0:T(2,128)} %bitcast.3, bf16[2048]{0:T(1024)(128)(2,1)} %norm_gain_ref.1, bf16[2048]{0:T(1024)(128)(2,1)} %passage_gain_ref.1, bf16[256]{0:T(256)(128)(2,1)} %key_gain_ref.1, bf16[256]{0:T(256)(128)(2,1)} %query_gain_ref.1, ...), custom_call_target="tpu_custom_call" | custom-call | flops 17179869184 | bytes 25165824 | tf_op jit(solution)/shard_map/layer/pallas_call | solution.py:747
  85.8 1.5 %add_parts.1 = bf16[512,2048]{1,0:T(8,128)(2,1)} custom-call(bf16[512,2048]{1,0:T(8,128)(2,1)S(1)} %get-tuple-element.7.keep_ref, bf16[512,2048]{1,0:T(8,128)(2,1)S(1)} %get-tuple-element.8.back_ref), custom_call_target="tpu_custom_call" | custom-call | tf_op jit(solution)/shard_map/add_parts/pallas_call | solution.py:637

commit v3 on v2

--- a/solution.py
+++ b/solution.py
@@ -133,6 +133,9 @@
     def reader_place(step):
         return p ^ step if power else (p + step) % plane
 
+    def asker_place(step):
+        return p ^ step if power else (p - step + plane) % plane
+
     far_planes = [o for o in range(depth) if max(o, depth - 1 - o) > REACH]
 
     def is_far(other):
@@ -210,66 +213,100 @@
     wanted_ref[...] = wanted
     own_ids = pltpu.make_async_copy(wanted_ref, wanted_smem, wanted_sem)
 
-    def project_passages(tile):
+    def project_passages(tile, before_keys=None, before_values=None):
         normed = row_norm(store_buf[tile], passage_gain_ref[...].astype(jnp.float32)[None, :])
-        keys = head_norm(dot32(normed, key_w[...]), key_gain_ref[...].astype(jnp.float32)[None, :])
+        if before_keys is not None:
+            before_keys()
+        key_gain = key_gain_ref[...].astype(jnp.float32)[None, :]
+        keys = head_norm(dot32(normed, key_w[...]), key_gain)
+        if before_values is not None:
+            before_values()
         values = dot32(normed, value_w[...]).astype(jnp.bfloat16)
         rows = pl.ds(tile * tile_passages, tile_passages)
         columns[0][rows, :, :width] = keys.reshape(tile_passages, passage_len, width)
         columns[0][rows, :, width:] = values.reshape(tile_passages, passage_len, width)
 
-    loads[0].wait()
-    loads[1].wait()
+    def first_loads():
+        loads[1].wait()
+        start_loads()
+
+    def start_loads():
+        for tile in range(1, tiles):
+            store_copy(tile).start()
+        x_copy.start()
+        for load in loads[2:]:
+            load.start()
+
     store_copy(0).wait()
-    for tile in range(1, tiles):
-        store_copy(tile).start()
-    x_copy.start()
-    for load in loads[2:]:
-        load.start()
-    project_passages(0)
+    project_passages(0, loads[0].wait, first_loads)
     pl.semaphore_wait(barrier, met)
 
-    def ids_copy(st, send_slot):
+    def far_row(other, home):
+        near = jnp.minimum(home, REACH) + REACH + 1
+        return jnp.where(other < home, other, jnp.maximum(other - near, 0))
+
+    def for_far(action):
+        for other in far_planes:
+
+            @pl.when(is_far(other))
+            def _(other=other):
+                action(other)
+
+    def ids_copy(st, row, send, recv):
         return pltpu.make_async_remote_copy(
             src_ref=wanted_ref,
-            dst_ref=ids_in.at[me],
-            send_sem=ids_send.at[send_slot],
-            recv_sem=ids_recv.at[me],
+            dst_ref=ids_in.at[row],
+            send_sem=ids_send.at[send],
+            recv_sem=ids_recv.at[recv],
             device_id=(st, tp),
             device_id_type=MESH,
         )
 
-    def ids_arrival(st):
+    def ids_rows(other):
+        if other is None:
+            return pl.ds(1, plane - 1), 0
+        row = far_row(other, z)
+        return pl.ds(plane * (1 + row), plane), 1 + row
+
+    def ids_all(other=None):
+        rows, sem = ids_rows(other)
         return pltpu.make_async_remote_copy(
-            src_ref=wanted_ref,
-            dst_ref=ids_in.at[st],
-            send_sem=ids_send.at[st],
-            recv_sem=ids_recv.at[st],
-            device_id=(st, tp),
+            src_ref=ids_in.at[rows],
+            dst_ref=ids_in.at[rows],
+            send_sem=ids_send.at[sem],
+            recv_sem=ids_recv.at[sem],
+            device_id=(me, 1 - tp),
             device_id_type=MESH,
         )
 
-    def ids_local(st):
-        return pltpu.make_async_copy(ids_in.at[st], ids_smem.at[st], ids_copy_sem.at[st])
-
-    def for_askers(action):
+    def ids_local(other=None):
+        rows, sem = ids_rows(other)
+        return pltpu.make_async_copy(ids_in.at[rows], ids_smem.at[rows], ids_copy_sem.at[sem])
+
+    def send_ids():
         for step in range(1, plane):
-            action(z * plane + reader_place(step))
-        for other in far_planes:
-
-            @pl.when(is_far(other))
-            def _(other=other):
-                for place in range(plane):
-                    action(other * plane + place)
-
-    def hop(level, up, tile):
+            ids_copy(z * plane + asker_place(step), step, 0, 0).start()
+
+        def send_far_ids(other):
+            there = far_row(z, other)
+            for step in range(plane):
+                ids_copy(
+                    other * plane + asker_place(step),
+                    plane * (1 + there) + step,
+                    1 + far_row(other, z),
+                    1 + there,
+                ).start()
+
+        for_far(send_far_ids)
+
+    def hop(level, up, tile, count=1):
         source = columns[-level if up else level]
         target = columns[-level - 1 if up else level + 1]
-        rows = pl.ds(tile * tile_passages, tile_passages)
+        rows = pl.ds(tile * tile_passages, count * tile_passages)
         return pltpu.make_async_remote_copy(
             src_ref=source.at[rows],
             dst_ref=target.at[rows],
-            send_sem=hop_send.at[level, int(up), tile],
+            send_sem=hop_send.at[level, int(up)],
             recv_sem=hop_recv.at[level, int(up), tile],
             device_id=(me + plane if up else me - plane, tp),
             device_id_type=MESH,
@@ -299,15 +336,15 @@
             def _(up=up):
                 hop(level, up, tile).wait_recv()
 
-    def end_hop(level, tile):
+    def end_hop(level):
         for up in (True, False):
 
             @pl.when(sends(level, up))
             def _(up=up):
-                hop(level, up, tile).wait_send()
+                hop(level, up, 0, tiles).wait_send()
 
     own_ids.start()
-    for_askers(lambda st: ids_copy(st, st).start())
+    send_ids()
     start_hop(0, 0)
 
     swap = pltpu.make_async_remote_copy(
@@ -326,21 +363,33 @@
         project_passages(tile)
         start_hop(0, tile)
 
-    def take_ids(st):
-        ids_arrival(st).wait_recv()
-        ids_local(st).start()
-
-    for_askers(take_ids)
-    for_askers(lambda st: ids_local(st).wait())
+    def take_ids(other=None):
+        ids_all(other).wait_recv()
+        ids_local(other).start()
+
+    take_ids()
+    for_far(take_ids)
+    ids_local().wait()
+    for_far(lambda other: ids_local(other).wait())
     own_ids.wait()
 
     def plane_copy(offset, step):
         return pltpu.make_async_remote_copy(
             src_ref=picked.at[offset + REACH, step - 1],
             dst_ref=slots.at[z + offset, step],
-            send_sem=plane_send.at[offset + REACH, step],
-            recv_sem=plane_recv.at[offset + REACH, step],
+            send_sem=plane_send.at[offset + REACH],
+            recv_sem=plane_recv.at[offset + REACH],
             device_id=(z * plane + reader_place(step), tp),
+            device_id_type=MESH,
+        )
+
+    def plane_all(offset):
+        return pltpu.make_async_remote_copy(
+            src_ref=picked.at[offset + REACH],
+            dst_ref=slots.at[z + offset, pl.ds(1, plane - 1)],
+            send_sem=plane_send.at[offset + REACH],
+            recv_sem=plane_recv.at[offset + REACH],
+            device_id=(me, 1 - tp),
             device_id_type=MESH,
         )
 
@@ -352,35 +401,40 @@
         def _():
             owner = (z + offset) * plane + p
             for step in range(plane - 1, -1, -1):
-                reader = z * plane + reader_place(step)
                 for rank in range(most):
                     entry = owner * most + rank
                     if step == 0:
                         index = wanted_smem[0, entry]
                         slots[z + offset, 0, rank] = columns[offset][index]
                     else:
-                        index = ids_smem[reader, 0, entry]
+                        index = ids_smem[step, 0, entry]
                         picked[offset + REACH, step - 1, rank] = columns[offset][index]
             for step in range(plane - 1, 0, -1):
                 plane_copy(offset, step).start()
 
-    def far_row(other):
-        near = jnp.minimum(z, REACH) + REACH + 1
-        return jnp.where(other < z, other, jnp.maximum(other - near, 0))
-
     def stage_copy(other, step):
         return pltpu.make_async_remote_copy(
-            src_ref=far_picked.at[far_row(other), step - 1],
-            dst_ref=far_stage.at[far_row(other), step],
-            send_sem=stage_send.at[far_row(other), step],
-            recv_sem=stage_recv.at[far_row(other), step],
+            src_ref=far_picked.at[far_row(other, z), step - 1],
+            dst_ref=far_stage.at[far_row(other, z), step],
+            send_sem=stage_send.at[far_row(other, z)],
+            recv_sem=stage_recv.at[far_row(other, z)],
             device_id=(z * plane + reader_place(step), tp),
             device_id_type=MESH,
         )
 
+    def stage_all(other):
+        return pltpu.make_async_remote_copy(
+            src_ref=far_picked.at[far_row(other, z)],
+            dst_ref=far_stage.at[far_row(other, z), pl.ds(1, plane - 1)],
+            send_sem=stage_send.at[far_row(other, z)],
+            recv_sem=stage_recv.at[far_row(other, z)],
+            device_id=(me, 1 - tp),
+            device_id_type=MESH,
+        )
+
     def far_copy(other, source):
         return pltpu.make_async_remote_copy(
-            src_ref=far_stage.at[far_row(other)],
+            src_ref=far_stage.at[far_row(other, z)],
             dst_ref=slots.at[source],
             send_sem=far_send.at[other],
             recv_sem=far_recv.at[source],
@@ -388,28 +442,20 @@
             device_id_type=MESH,
         )
 
-    def for_far(action):
-        for other in far_planes:
-
-            @pl.when(is_far(other))
-            def _(other=other):
-                action(other)
-
     def stage_far(other):
         for step in range(plane - 1, -1, -1):
-            reader = other * plane + reader_place(step)
+            row = plane * (1 + far_row(other, z)) + step
             for rank in range(most):
-                block = columns[0][ids_smem[reader, 0, me * most + rank]]
+                block = columns[0][ids_smem[row, 0, me * most + rank]]
                 if step == 0:
-                    far_stage[far_row(other), 0, rank] = block
+                    far_stage[far_row(other, z), 0, rank] = block
                 else:
-                    far_picked[far_row(other), step - 1, rank] = block
+                    far_picked[far_row(other, z), step - 1, rank] = block
         for step in range(plane - 1, 0, -1):
             stage_copy(other, step).start()
 
     def send_far(other):
-        for step in range(1, plane):
-            stage_copy(other, step).wait_recv()
+        stage_all(other).wait_recv()
         far_copy(other, z).start()
 
     deliver(0)
@@ -533,17 +579,18 @@
 
         @pl.when(held(offset))
         def _(offset=offset):
-            for step in range(1, plane):
-                plane_copy(offset, step).wait_recv()
+            plane_all(offset).wait_recv()
 
     for_far(lambda other: far_copy(other, other).wait_recv())
 
-    heads = width // MEM_HD
     blocks = slots_ref.shape[0] // passes
     block = tokens // blocks
-    head_of = lax.broadcasted_iota(jnp.int32, (heads * block, width), 1) // MEM_HD
-    row_head = lax.broadcasted_iota(jnp.int32, (heads * block, width), 0) // block
-    inside = head_of == row_head
+    lanes = min(128, width)
+    per_tile = lanes // MEM_HD
+    read_rows = passes * passage_len
+    lane_head = lax.broadcasted_iota(jnp.int32, (read_rows, lanes), 1) // MEM_HD
+    of_head = [lane_head == head for head in range(per_tile)]
+    ones = [jnp.where(inside, 1.0, 0.0).astype(jnp.bfloat16) for inside in of_head]
     gate = jnp.tanh(gate_ref[...].astype(jnp.float32)[None, :])
 
     def attend(first, count):
@@ -552,24 +599,43 @@
             index = first + number
             rows = pl.ds(pl.multiple_of(index * block, block), block)
             query = queries[rows, :]
-            stacked = jnp.concatenate([query] * heads, axis=0)
-            stacked = jnp.where(inside, stacked, jnp.zeros_like(stacked))
             read = []
             for part in range(passes):
                 slot = slots_ref[index * passes + part]
                 read.append(slots[slot // (plane * most), slot // most % plane, slot % most])
-            keys = jnp.concatenate([part[:, :width] for part in read], axis=0)
-            values = jnp.concatenate([part[:, width:] for part in read], axis=0)
-            scores = lax.dot_general(
-                stacked, keys, (((1,), (1,)), ((), ())), preferred_element_type=jnp.float32
-            ) * MEM_HD ** (-0.5)
-            expanded = jnp.exp(scores - jnp.max(scores, axis=-1, keepdims=True))
-            weights = (expanded / jnp.sum(expanded, axis=-1, keepdims=True)).astype(jnp.bfloat16)
-            mixed = jnp.where(inside, dot32(weights, values), 0.0)
-            attended = mixed[:block]
-            for head in range(1, heads):
-                attended = attended + mixed[head * block : (head + 1) * block]
-            memory[rows, :] = (attended * gate).astype(jnp.bfloat16)
+            for left in range(0, width, lanes):
+                keys = jnp.concatenate([part[:, left : left + lanes] for part in read], axis=0)
+                values = jnp.concatenate(
+                    [part[:, width + left : width + left + lanes] for part in read], axis=0
+                )
+                zeros = jnp.zeros_like(keys)
+                split_keys = jnp.concatenate(
+                    [jnp.where(inside, keys, zeros) for inside in of_head], axis=0
+                )
+                scores = lax.dot_general(
+                    query[:, left : left + lanes],
+                    split_keys,
+                    (((1,), (1,)), ((), ())),
+                    preferred_element_type=jnp.float32,
+                )
+                expanded = []
+                for head in range(per_tile):
+                    mine = scores[:, head * read_rows : (head + 1) * read_rows]
+                    top = jnp.max(mine, axis=-1, keepdims=True)
+                    expanded.append(jnp.exp((mine - top) * MEM_HD ** (-0.5)))
+                weights = jnp.concatenate(expanded, axis=1).astype(jnp.bfloat16)
+                split_values = jnp.concatenate(
+                    [
+                        jnp.concatenate([jnp.where(inside, values, zeros), one], axis=1)
+                        for inside, one in zip(of_head, ones)
+                    ],
+                    axis=0,
+                )
+                mixed = dot32(weights, split_values)
+                attended = mixed[:, :lanes] / mixed[:, lanes:]
+                memory[rows, left : left + lanes] = (
+                    attended * gate[:, left : left + lanes]
+                ).astype(jnp.bfloat16)
 
     share = tokens // 2
     pieces = tp_send.shape[0] - 2
@@ -593,20 +659,18 @@
     def _(number):
         keep_ref[pl.ds(pl.multiple_of(number * piece, piece), piece), :] = part_of(tp, number)
 
-    for_askers(lambda st: ids_copy(st, st).wait_send())
+    ids_all().wait_send()
+    for_far(lambda other: ids_all(other).wait_send())
     for level in range(REACH):
-        for tile in range(tiles):
-            end_hop(level, tile)
+        end_hop(level)
     for offset in OFFSETS:
 
         @pl.when(held(offset))
         def _(offset=offset):
-            for step in range(1, plane):
-                plane_copy(offset, step).wait_send()
+            plane_all(offset).wait_send()
 
     def end_far(other):
-        for step in range(1, plane):
-            stage_copy(other, step).wait_send()
+        stage_all(other).wait_send()
         far_copy(other, z).wait_send()
 
     for_far(end_far)
@@ -716,8 +780,8 @@
             pltpu.VMEM((1, wide), jnp.int32),
             pltpu.SMEM((1, wide), jnp.int32),
             pltpu.SMEM((request_count,), jnp.int32),
-            pltpu.VMEM((owner_count, 1, wide), jnp.int32),
-            pltpu.SMEM((owner_count, 1, wide), jnp.int32),
+            pltpu.VMEM(((1 + far_rows) * plane, 1, wide), jnp.int32),
+            pltpu.SMEM(((1 + far_rows) * plane, 1, wide), jnp.int32),
             pltpu.VMEM((depth, plane, most) + row, bf16),
         ]
         + [pltpu.VMEM((store_size,) + row, bf16) for _ in OFFSETS]
@@ -729,15 +793,15 @@
             dma((tiles,)),
             dma,
             dma,
-            dma((owner_count,)),
-            dma((owner_count,)),
-            dma((owner_count,)),
+            dma((1 + far_rows,)),
+            dma((1 + far_rows,)),
+            dma((1 + far_rows,)),
+            dma((REACH, 2)),
             dma((REACH, 2, tiles)),
-            dma((REACH, 2, tiles)),
-            dma((reach, plane)),
-            dma((reach, plane)),
-            dma((far_rows, plane)),
-            dma((far_rows, plane)),
+            dma((reach,)),
+            dma((reach,)),
+            dma((far_rows,)),
+            dma((far_rows,)),
             dma((depth,)),
             dma((depth,)),
             dma((2 + pieces,)),

time: 87.4 us -> 85.4 us (0.977)
  Pallas kernels: 87.2 us -> 85.3 us
    pallas_call x1, Pallas kernels: 85.8 us -> 83.8 us  [layer(): pl.pallas_call(functools.partial(layer_kernel, depth, plane, most, passag...]
where the time goes in v3:
time: 85.4 us; the launch traced here: 85.3 us
  Pallas kernels  85.3 us (100%)
    pallas_call x1, Pallas kernels, layer(): pl.pallas_call(functools.partial(layer_kernel, depth, plane, most, passag...  83.8 us

profile of v3, /device:TPU:0, one launch (start us, length us, event | category | flops | bytes accessed | tf_op | source)
XLA Modules:
  0.0 85.3 jit_solution(1899485140411168229)
XLA Ops:
  0.0 83.8 %layer.1 = (bf16[512,2048]{1,0:T(8,128)(2,1)S(1)}, bf16[512,2048]{1,0:T(8,128)(2,1)S(1)}) custom-call(s32[2,16]{1,0:T(2,128)} %bitcast.3, bf16[2048]{0:T(1024)(128)(2,1)} %norm_gain_ref.1, bf16[2048]{0:T(1024)(128)(2,1)} %passage_gain_ref.1, bf16[256]{0:T(256)(128)(2,1)} %key_gain_ref.1, bf16[256]{0:T(256)(128)(2,1)} %query_gain_ref.1, ...), custom_call_target="tpu_custom_call" | custom-call | flops 17179869184 | bytes 25165824 | tf_op jit(solution)/shard_map/layer/pallas_call | solution.py:811
  83.8 1.5 %add_parts.1 = bf16[512,2048]{1,0:T(8,128)(2,1)} custom-call(bf16[512,2048]{1,0:T(8,128)(2,1)S(1)} %get-tuple-element.7.keep_ref, bf16[512,2048]{1,0:T(8,128)(2,1)S(1)} %get-tuple-element.8.back_ref), custom_call_target="tpu_custom_call" | custom-call | tf_op jit(solution)/shard_map/add_parts/pallas_call | solution.py:701

commit v4 on v3

--- a/solution.py
+++ b/solution.py
@@ -213,32 +213,28 @@
     wanted_ref[...] = wanted
     own_ids = pltpu.make_async_copy(wanted_ref, wanted_smem, wanted_sem)
 
-    def project_passages(tile, before_keys=None, before_values=None):
-        normed = row_norm(store_buf[tile], passage_gain_ref[...].astype(jnp.float32)[None, :])
-        if before_keys is not None:
-            before_keys()
+    def project_passages(tile, part=0, parts=1):
+        taken = tile_rows // parts
+        raw = store_buf[tile, part * taken : (part + 1) * taken]
+        normed = row_norm(raw, passage_gain_ref[...].astype(jnp.float32)[None, :])
         key_gain = key_gain_ref[...].astype(jnp.float32)[None, :]
         keys = head_norm(dot32(normed, key_w[...]), key_gain)
-        if before_values is not None:
-            before_values()
         values = dot32(normed, value_w[...]).astype(jnp.bfloat16)
-        rows = pl.ds(tile * tile_passages, tile_passages)
-        columns[0][rows, :, :width] = keys.reshape(tile_passages, passage_len, width)
-        columns[0][rows, :, width:] = values.reshape(tile_passages, passage_len, width)
-
-    def first_loads():
-        loads[1].wait()
-        start_loads()
-
-    def start_loads():
-        for tile in range(1, tiles):
-            store_copy(tile).start()
-        x_copy.start()
-        for load in loads[2:]:
-            load.start()
-
+        count = tile_passages // parts
+        rows = pl.ds(tile * tile_passages + part * count, count)
+        columns[0][rows, :, :width] = keys.reshape(count, passage_len, width)
+        columns[0][rows, :, width:] = values.reshape(count, passage_len, width)
+
+    loads[0].wait()
+    loads[1].wait()
     store_copy(0).wait()
-    project_passages(0, loads[0].wait, first_loads)
+    for tile in range(1, tiles):
+        store_copy(tile).start()
+    x_copy.start()
+    for load in loads[2:]:
+        load.start()
+    first_parts = 2 if tile_passages % 2 == 0 else 1
+    project_passages(0, 0, first_parts)
     pl.semaphore_wait(barrier, met)
 
     def far_row(other, home):
@@ -299,10 +295,11 @@
 
         for_far(send_far_ids)
 
-    def hop(level, up, tile, count=1):
+    def hop(level, up, tile, count=1, part=0, parts=1):
         source = columns[-level if up else level]
         target = columns[-level - 1 if up else level + 1]
-        rows = pl.ds(tile * tile_passages, count * tile_passages)
+        taken = count * tile_passages // parts
+        rows = pl.ds(tile * tile_passages + part * taken, taken)
         return pltpu.make_async_remote_copy(
             src_ref=source.at[rows],
             dst_ref=target.at[rows],
@@ -322,12 +319,12 @@
             return z >= level + 1
         return z <= depth - 2 - level
 
-    def start_hop(level, tile):
+    def start_hop(level, tile, part=0, parts=1):
         for up in (True, False):
 
             @pl.when(sends(level, up))
             def _(up=up):
-                hop(level, up, tile).start()
+                hop(level, up, tile, 1, part, parts).start()
 
     def await_hop(level, tile):
         for up in (True, False):
@@ -345,7 +342,10 @@
 
     own_ids.start()
     send_ids()
-    start_hop(0, 0)
+    start_hop(0, 0, 0, first_parts)
+    for part in range(1, first_parts):
+        project_passages(0, part, first_parts)
+        start_hop(0, 0, part, first_parts)
 
     swap = pltpu.make_async_remote_copy(
         src_ref=tokens_hbm,
@@ -640,23 +640,30 @@
     share = tokens // 2
     pieces = tp_send.shape[0] - 2
     piece, few = share // pieces, blocks // 2 // pieces
+    subs = 2
+    few_rows = piece // subs
 
     def part_copy(number):
         rows = pl.ds(pl.multiple_of(number * piece, piece), piece)
         return tp_copy(2 + number, x_buf.at[rows], back_ref.at[rows])
 
-    def part_of(core, number):
-        attend(core * (blocks // 2) + number * few, few)
-        rows = pl.ds(pl.multiple_of(core * share + number * piece, piece), piece)
+    def part_of(core, number, sub=0, subs=1):
+        few_rows = piece // subs
+        start = core * share + number * piece + sub * few_rows
+        rows = pl.ds(pl.multiple_of(start, few_rows), few_rows)
         return (acc[rows, :] + dot32(memory[rows, :], mem_out_w[...])).astype(jnp.bfloat16)
 
     @pl.loop(0, pieces)
     def _(number):
-        x_buf[pl.ds(pl.multiple_of(number * piece, piece), piece), :] = part_of(1 - tp, number)
-        part_copy(number).start()
+        attend((1 - tp) * (blocks // 2) + number * few, few)
+        for sub in range(subs):
+            rows = pl.ds(pl.multiple_of(number * piece + sub * few_rows, few_rows), few_rows)
+            x_buf[rows, :] = part_of(1 - tp, number, sub, subs)
+            tp_copy(2 + number, x_buf.at[rows], back_ref.at[rows]).start()
 
     @pl.loop(0, pieces)
     def _(number):
+        attend(tp * (blocks // 2) + number * few, few)
         keep_ref[pl.ds(pl.multiple_of(number * piece, piece), piece), :] = part_of(tp, number)
 
     ids_all().wait_send()

time: 85.4 us -> 84.4 us (0.988)
  Pallas kernels: 85.3 us -> 84.2 us
    pallas_call x1, Pallas kernels: 83.8 us -> 82.8 us  [layer(): pl.pallas_call(functools.partial(layer_kernel, depth, plane, most, passag...]
where the time goes in v4:
time: 84.4 us; the launch traced here: 84.3 us
  Pallas kernels  84.2 us (100%)
    pallas_call x1, Pallas kernels, layer(): pl.pallas_call(functools.partial(layer_kernel, depth, plane, most, passag...  82.8 us

profile of v4, /device:TPU:0, one launch (start us, length us, event | category | flops | bytes accessed | tf_op | source)
XLA Modules:
  0.0 84.3 jit_solution(8007925045771367823)
XLA Ops:
  0.0 82.8 %layer.1 = (bf16[512,2048]{1,0:T(8,128)(2,1)S(1)}, bf16[512,2048]{1,0:T(8,128)(2,1)S(1)}) custom-call(s32[2,16]{1,0:T(2,128)} %bitcast.3, bf16[2048]{0:T(1024)(128)(2,1)} %norm_gain_ref.1, bf16[2048]{0:T(1024)(128)(2,1)} %passage_gain_ref.1, bf16[256]{0:T(256)(128)(2,1)} %key_gain_ref.1, bf16[256]{0:T(256)(128)(2,1)} %query_gain_ref.1, ...), custom_call_target="tpu_custom_call" | custom-call | flops 17179869184 | bytes 25165824 | tf_op jit(solution)/shard_map/layer/pallas_call | solution.py:818
  82.8 1.5 %add_parts.1 = bf16[512,2048]{1,0:T(8,128)(2,1)} custom-call(bf16[512,2048]{1,0:T(8,128)(2,1)S(1)} %get-tuple-element.7.keep_ref, bf16[512,2048]{1,0:T(8,128)(2,1)S(1)} %get-tuple-element.8.back_ref), custom_call_target="tpu_custom_call" | custom-call | tf_op jit(solution)/shard_map/add_parts/pallas_call | solution.py:708

commit v5 on v4

--- a/solution.py
+++ b/solution.py
@@ -309,6 +309,33 @@
             device_id_type=MESH,
         )
 
+    def last_piece(level, up, tail):
+        kept = tile_passages - 1
+        start = (tiles - 1) * tile_passages + (kept if tail else 0)
+        rows = pl.ds(start, 1 if tail else kept)
+        return pltpu.make_async_remote_copy(
+            src_ref=columns[-level if up else level].at[rows],
+            dst_ref=columns[-level - 1 if up else level + 1].at[rows],
+            send_sem=hop_send.at[level, int(up)],
+            recv_sem=hop_recv.at[level, int(up), tiles if tail else tiles - 1],
+            device_id=(me + plane if up else me - plane, tp),
+            device_id_type=MESH,
+        )
+
+    def for_hops(level, chosen, action):
+        for up in (True, False):
+
+            @pl.when(chosen(level, up))
+            def _(up=up):
+                action(up)
+
+    def start_last(level):
+        def both(up):
+            last_piece(level, up, False).start()
+            last_piece(level, up, True).start()
+
+        for_hops(level, sends, both)
+
     def sends(level, up):
         if up:
             return (z >= level) & (z < depth - 1)
@@ -522,7 +549,10 @@
     convolve(0)
     for tile in range(min(token_tiles, tiles - 1), tiles):
         await_hop(0, tile)
-        start_hop(1, tile)
+        if tile < tiles - 1:
+            start_hop(1, tile)
+        else:
+            start_last(1)
     for distance in range(1, 2):
         deliver(-distance)
         deliver(distance)
@@ -569,12 +599,14 @@
         )
         acc[rows, :] = dot32(jax.nn.silu(scaled).astype(jnp.bfloat16), conv_out_w[...])
 
-    for tile in range(tiles):
+    for tile in range(tiles - 1):
         await_hop(1, tile)
+    for_hops(1, gets, lambda up: last_piece(1, up, False).wait_recv())
+    for_far(send_far)
+    for_hops(1, gets, lambda up: last_piece(1, up, True).wait_recv())
     for distance in range(2, REACH + 1):
         deliver(-distance)
         deliver(distance)
-    for_far(send_far)
     for offset in OFFSETS:
 
         @pl.when(held(offset))
@@ -804,7 +836,7 @@
             dma((1 + far_rows,)),
             dma((1 + far_rows,)),
             dma((REACH, 2)),
-            dma((REACH, 2, tiles)),
+            dma((REACH, 2, tiles + 1)),
             dma((reach,)),
             dma((reach,)),
             dma((far_rows,)),

time: 84.4 us -> 83 us (0.983)
  Pallas kernels: 84.2 us -> 82.8 us
    pallas_call x1, Pallas kernels: 82.8 us -> 81.3 us  [layer(): pl.pallas_call(functools.partial(layer_kernel, depth, plane, most, passag...]
where the time goes in v5:
time: 83 us; the launch traced here: 82.8 us
  Pallas kernels  82.8 us (100%)
    pallas_call x1, Pallas kernels, layer(): pl.pallas_call(functools.partial(layer_kernel, depth, plane, most, passag...  81.3 us

profile of v5, /device:TPU:0, one launch (start us, length us, event | category | flops | bytes accessed | tf_op | source)
XLA Modules:
  0.0 82.8 jit_solution(745170208762919770)
XLA Ops:
  0.0 81.3 %layer.1 = (bf16[512,2048]{1,0:T(8,128)(2,1)S(1)}, bf16[512,2048]{1,0:T(8,128)(2,1)S(1)}) custom-call(s32[2,16]{1,0:T(2,128)} %bitcast.3, bf16[2048]{0:T(1024)(128)(2,1)} %norm_gain_ref.1, bf16[2048]{0:T(1024)(128)(2,1)} %passage_gain_ref.1, bf16[256]{0:T(256)(128)(2,1)} %key_gain_ref.1, bf16[256]{0:T(256)(128)(2,1)} %query_gain_ref.1, ...), custom_call_target="tpu_custom_call" | custom-call | flops 17179869184 | bytes 25165824 | tf_op jit(solution)/shard_map/layer/pallas_call | solution.py:850
  81.3 1.5 %add_parts.1 = bf16[512,2048]{1,0:T(8,128)(2,1)} custom-call(bf16[512,2048]{1,0:T(8,128)(2,1)S(1)} %get-tuple-element.7.keep_ref, bf16[512,2048]{1,0:T(8,128)(2,1)S(1)} %get-tuple-element.8.back_ref), custom_call_target="tpu_custom_call" | custom-call | tf_op jit(solution)/shard_map/add_parts/pallas_call | solution.py:740
